TPU v7x, 32 devices: a whole 2x2x4 slice. The times are simulated.
32 devices in a mesh: grp: 2 (over y), sp: 4 (over z), tp: 4 (over x, core).
Axes of the slice: x: 2, y: 2, z: 4, core: 2. Of those that a mesh axis runs over, the one named last changes fastest.
Arguments:
- queries: bfloat16 [4096, 1024], P(('grp', 'sp'), 'tp'), parts along dimension 0, may hold values from -6 to 6
- keys: bfloat16 [4096, 1024], P(('grp', 'sp'), 'tp'), parts along dimension 0, may hold values from -6 to 6
- values: bfloat16 [4096, 2048], P(('grp', 'sp'), 'tp'), parts along dimension 0, may hold values from -6 to 6
- in_gate: float32 [8, 4096], P('tp', ('grp', 'sp')), parts along dimension 1, may hold values from -4 to 220
- forget_gate: float32 [8, 4096], P('tp', ('grp', 'sp')), parts along dimension 1, may hold values from 0 to 16
- head_gain: float32 [2048], P('tp'), may hold values from 0.1 to 1.9
- out_weight: bfloat16 [2048, 2048], P('tp'), may hold values from -0.125 to 0.125
- resid: bfloat16 [4096, 2048], P(('grp', 'sp', 'tp')), parts along dimension 0, may hold values from -6 to 6
- norm_gain: float32 [2048], replicated, may hold values from 0.1 to 1.9
- expert_ids: int32 [4096, 2], P(('grp', 'sp', 'tp')), parts along dimension 0, may hold values from 0 to 15, all different within a row; in each aligned block of 128 rows (0 to 127, 128 to 255, ...) at most 64 rows name the same one
- expert_mix: float32 [4096, 2], P(('grp', 'sp', 'tp')), parts along dimension 0, may hold values from 0.25 to 1
- gate_weight: bfloat16 [16, 2048, 512], P(('sp', 'tp')), may hold values from -0.125 to 0.125
- up_weight: bfloat16 [16, 2048, 512], P(('sp', 'tp')), may hold values from -0.125 to 0.125
- down_weight: bfloat16 [16, 512, 2048], P(('sp', 'tp')), may hold values from -0.25 to 0.25
Outputs:
- final: bfloat16 [4096, 2048], P(('grp', 'sp', 'tp')), parts along dimension 0
There are 2 independent parts, one for each index of `grp`. A program takes and returns all parts, laid end to end along the dimension named above; an argument that names none is the same for every part. Nothing has to cross between parts.
Inputs may be any that keep to these rules, and one draw needn't show every extreme that they name: `expert_ids`: each row names 2 different experts. In each aligned block of 128 rows (the rows of one device) no expert is named more than 64 times, a bound that some block reaches.
All inputs are finite; a program needn't handle non-finite values.
Results may differ from a plain program's by a relative error of at most 0.013.
Values may be sent and summed in bfloat16 or wider, within the bound.
A program may use at most 128 MiB of HBM per device.

v0:
```python
import jax
import jax.numpy as jnp
from jax import lax
from jax.sharding import PartitionSpec as P

QK_HEAD = 128
V_HEAD = 256
BLOCK = 128
TOPK = 2
CAP_FACTOR = 4


EPSILON = 1e-06
VERY_LOW = -1e30


def entering(x, axis, combine, identity):
    count, position = (lax.axis_size(axis), lax.axis_index(axis))
    everything = jax.tree.map(lambda part: lax.all_gather(part, axis), x)
    start = jax.tree.map(
        lambda part, zero: jnp.broadcast_to(jnp.asarray(zero, part.dtype), part.shape), x, identity
    )

    def hop(k, before):
        reached = k < position
        new = combine(before, jax.tree.map(lambda part: part[k], everything))
        return jax.tree.map(lambda a, b: jnp.where(reached, a, b), new, before)

    return lax.fori_loop(0, count, hop, start)


def join_states(before_part, after_part):
    before_total, before_state, before_stab = before_part
    after_total, after_state, after_stab = after_part
    stab = jnp.maximum(before_stab + after_total, after_stab)
    keep = jnp.exp(before_stab + after_total - stab)
    added = jnp.exp(after_stab - stab)
    return (
        before_total + after_total,
        before_state * keep[:, None, None] + after_state * added[:, None, None],
        stab,
    )


def expert_ffn(arrived, gate_weight, up_weight, down_weight):
    width = arrived.shape[-1]
    flat = arrived.reshape(-1, width)
    gate = jnp.dot(flat, gate_weight[0], preferred_element_type=jnp.float32)
    upper = jnp.dot(flat, up_weight[0], preferred_element_type=jnp.float32)
    hidden = (jax.nn.silu(gate) * upper).astype(jnp.bfloat16)
    output = jnp.dot(hidden, down_weight[0], preferred_element_type=jnp.float32).astype(
        jnp.bfloat16
    )
    return output.reshape(arrived.shape)


def per_device(
    queries,
    keys,
    values,
    in_gate,
    forget_gate,
    head_gain,
    out_weight,
    resid,
    norm_gain,
    expert_ids,
    expert_mix,
    gate_weight,
    up_weight,
    down_weight,
):
    tokens = queries.shape[0]
    heads = in_gate.shape[0]
    count = tokens // BLOCK
    scale = QK_HEAD ** (-0.5)
    query_tiles = queries.reshape(count, BLOCK, heads, QK_HEAD)
    key_blocks = keys.reshape(count, BLOCK, heads, QK_HEAD)
    value_tiles = values.reshape(count, BLOCK, heads, V_HEAD)
    in_blocks = in_gate.reshape(heads, count, BLOCK)
    cumulative = jnp.cumsum(jax.nn.log_sigmoid(forget_gate).reshape(heads, count, BLOCK), axis=2)
    totals = cumulative[:, :, -1]
    to_end = totals[:, :, None] - cumulative + in_blocks
    end_max = jnp.max(to_end, axis=2)
    end_weight = jnp.exp(to_end - end_max[:, :, None]).transpose(1, 2, 0)
    key_weighted = (key_blocks * end_weight[..., None]).astype(jnp.bfloat16)
    state_per_block = jnp.einsum(
        "clhv,clhk->hcvk", value_tiles, key_weighted, preferred_element_type=jnp.float32
    )
    summary = (totals[:, 0], state_per_block[:, 0], end_max[:, 0])
    for block_no in range(1, count):
        summary = join_states(
            summary, (totals[:, block_no], state_per_block[:, block_no], end_max[:, block_no])
        )
    identity = (
        jnp.zeros_like(summary[0]),
        jnp.zeros_like(summary[1]),
        jnp.full_like(summary[2], VERY_LOW),
    )
    prefix = entering(summary, "sp", join_states, identity)
    enter_stab = jnp.maximum(prefix[0], prefix[2])
    factor = jnp.exp(prefix[2] - enter_stab)
    enter_state = prefix[1] * factor[:, None, None]
    state, stab = (enter_state, enter_stab)
    state_list, stab_list = ([], [])
    for block_no in range(count):
        state_list.append(state)
        stab_list.append(stab)
        new_stab = jnp.maximum(totals[:, block_no] + stab, end_max[:, block_no])
        keep = jnp.exp(totals[:, block_no] + stab - new_stab)
        added = jnp.exp(end_max[:, block_no] - new_stab)
        state = state * keep[:, None, None] + state_per_block[:, block_no] * added[:, None, None]
        stab = new_stab
    prev_state = jnp.stack(state_list, axis=1)
    prev_stab = jnp.stack(stab_list, axis=1)
    scores = (
        jnp.einsum("cthd,cshd->hcts", query_tiles, key_blocks, preferred_element_type=jnp.float32)
        * scale
    )
    causal = jnp.tril(jnp.ones((BLOCK, BLOCK), dtype=bool))
    gaps = cumulative[..., :, None] - cumulative[..., None, :] + in_blocks[..., None, :]
    gaps = jnp.where(causal, gaps, -jnp.inf)
    row_max = jnp.max(gaps, axis=3)
    weights = scores * jnp.exp(gaps - row_max[..., None])
    rounded = weights.astype(jnp.bfloat16)
    local_num = jnp.einsum(
        "hcts,cshv->hctv", rounded, value_tiles, preferred_element_type=jnp.float32
    )
    inter = cumulative + prev_stab[..., None]
    stab_t = jnp.maximum(inter, row_max)
    own_scale = jnp.exp(row_max - stab_t)
    carried = jnp.exp(inter - stab_t)
    query_scaled = query_tiles.astype(jnp.float32) * scale
    memory_readout = jnp.einsum(
        "cthk,hcvk->hctv", query_scaled, prev_state, precision=lax.Precision.HIGHEST
    )
    cell = own_scale[..., None] * local_num + carried[..., None] * memory_readout
    cell = cell * lax.rsqrt(jnp.mean(cell * cell, axis=3, keepdims=True) + EPSILON)
    cell = cell * head_gain.reshape(heads, 1, 1, V_HEAD)
    mixed = cell.transpose(1, 2, 0, 3).reshape(tokens, heads * V_HEAD).astype(jnp.bfloat16)
    shard = tokens // lax.axis_size("tp")
    proj = lax.psum_scatter(
        jnp.dot(mixed, out_weight, preferred_element_type=jnp.float32).astype(jnp.bfloat16),
        "tp",
        scatter_dimension=0,
        tiled=True,
    ).astype(jnp.float32)
    mid_f = (resid.astype(jnp.float32) + proj).astype(jnp.bfloat16).astype(jnp.float32)
    normed = (
        mid_f * lax.rsqrt(jnp.mean(mid_f * mid_f, axis=1, keepdims=True) + EPSILON) * norm_gain
    ).astype(jnp.bfloat16)
    width = normed.shape[1]
    expert_group = lax.axis_size("sp") * lax.axis_size("tp")
    assigns = expert_ids.reshape(-1)
    assign_count = assigns.shape[0]
    slots_each = CAP_FACTOR * assign_count // expert_group
    one_hot = (assigns[:, None] == jnp.arange(expert_group, dtype=jnp.int32)[None, :]).astype(
        jnp.bfloat16
    )
    earlier_mask = jnp.tril(jnp.ones((assign_count, assign_count), jnp.bfloat16), -1)
    counts_before = jnp.dot(earlier_mask, one_hot, preferred_element_type=jnp.float32)
    slot = jnp.sum(counts_before * one_hot.astype(jnp.float32), axis=1).astype(jnp.int32)
    target = assigns * slots_each + slot
    filler = (
        jnp.full((expert_group * slots_each,), -1, jnp.int32)
        .at[target]
        .set(jnp.arange(assign_count, dtype=jnp.int32))
    )
    rows_from = jnp.maximum(filler, 0) // TOPK
    outgoing = jnp.where((filler >= 0)[:, None], normed[rows_from], jnp.zeros((), jnp.bfloat16))
    outgoing = outgoing.reshape(expert_group, slots_each, width)
    served = expert_ffn(
        lax.all_to_all(outgoing, ("sp", "tp"), split_axis=0, concat_axis=0, tiled=True),
        gate_weight,
        up_weight,
        down_weight,
    )
    returned = lax.all_to_all(served, ("sp", "tp"), split_axis=0, concat_axis=0, tiled=True)
    picked = returned.reshape(expert_group * slots_each, width)[target]
    picked = picked.reshape(shard, TOPK, width).astype(jnp.float32)
    share = expert_mix / jnp.sum(expert_mix, axis=1, keepdims=True)
    total = jnp.sum(share[:, :, None] * picked, axis=1)
    return (mid_f + total).astype(jnp.bfloat16)


def solution(mesh):
    in_specs = (
        P(("grp", "sp"), "tp"),
        P(("grp", "sp"), "tp"),
        P(("grp", "sp"), "tp"),
        P("tp", ("grp", "sp")),
        P("tp", ("grp", "sp")),
        P("tp"),
        P("tp", None),
        P(("grp", "sp", "tp"), None),
        P(),
        P(("grp", "sp", "tp"), None),
        P(("grp", "sp", "tp"), None),
        P(("sp", "tp"), None, None),
        P(("sp", "tp"), None, None),
        P(("sp", "tp"), None, None),
    )
    out_specs = P(("grp", "sp", "tp"), None)
    return jax.shard_map(
        per_device, mesh=mesh, in_specs=in_specs, out_specs=out_specs, check_vma=False
    )
```

profile of v0, /device:TPU:11, one launch (start us, length us, event | category | flops | bytes accessed | tf_op | source)
XLA Modules:
  0.0 335.8 jit_solution(1238197305617205747)
XLA Ops:
  6.5 0.9 fusion.69
  7.4 0.6 reduce_window_sum.13
  8.0 0.2 slice_reduce_fusion
  8.2 0.7 add.331
  9.1 0.3 slice_reduce_fusion.6
  9.5 1.0 reshape.410
  10.5 0.2 copy.44
  10.7 2.1 reshape.411
  12.8 1.3 convolution_bitcast_fusion
  14.2 0.8 fusion.36
  15.0 1.8 copy.49
  16.9 0.7 dynamic-slice
  18.2 0.2 dynamic-update-slice
  18.5 0.2 dynamic-update-slice.1
  18.7 7.2 %all-reduce.2 = (f32[8]{0:T(128)S(1)}, f32[8]{0:T(128)S(1)}) all-reduce(f32[8]{0:T(128)S(1)} %dynamic-update-slice, f32[8]{0:T(128)S(1)} %dynamic-update-slice.1), channel_id=2, replica_groups=mesh['grp'=2,'sp'=4,'tp'=4] {'sp'}, use_global_device_ids=true, to_apply=%add | all-reduce | flops 16 | bytes 128
  26.1 1.7 reshape.412
  27.9 0.4 fusion.32
  28.3 2.8 fusion.14
  31.0 14.6 %all-gather.4.cloned.1.call-done = f32[4,2,256,128]{3,2,1,0:T(8,128)} async-done(((f32[1,2,256,128]{3,2,1,0:T(8,128)}), f32[4,2,256,128]{3,2,1,0:T(8,128)}) %all-gather.4.cloned.1.call-update) | async-done | bytes 1048592 | tf_op jit(solution)/shard_map/all_gather | solution.py:19
  45.6 4.5 %while.18 = (s32[]{:T(128)}, f32[2]{0:T(128)S(1)}, f32[2,256,128]{2,1,0:T(8,128)S(1)}, f32[2]{0:T(128)S(1)}, s32[]{:T(128)}, /*index=5*/f32[4,2]{1,0:T(4,128)S(1...) while((s32[]{:T(128)}, f32[2]{0:T(128)S(1)}, ...), condition=%wide.region_4.5_spmd.clone, body=%wide.region_3.4_spmd.clone.sunk | while | flops 327704 | bytes 786671 | solution.py:29
  45.7 1.1 fusion.92
  46.8 1.1 fusion.92
  47.9 1.1 fusion.92
  49.1 1.1 fusion.92
  50.2 0.8 copy.55
  51.2 1.2 fusion.83
  52.6 2.2 multiply_reduce_fusion.1
  55.0 1.9 fusion.23
  56.8 0.5 copy.58
  57.5 2.6 convolution_convert_fusion.1
  60.1 0.6 copy-done.9
  61.0 0.3 fusion.15
  61.6 1.4 scatter_custom_fusion
  63.1 27.1 %reduce-scatter.2.cloned.1.call-done = bf16[128,2048]{1,0:T(8,128)(2,1)} async-done(((bf16[512,2048]{1,0:T(8,128)(2,1)}), bf16[128,2048]{1,0:T(8,128)(2,1)}) %reduce-scatter.2.cloned.1.call-update) | async-done | bytes 524304 | tf_op jit(solution)/shard_map/reduce_scatter | solution.py:142
  90.3 1.3 fusion.16
  91.6 1.3 fusion.18
  92.9 6.0 %gather_fusion = bf16[1024,2048]{1,0:T(8,128)(2,1)} fusion(bf16[128,2048]{1,0:T(8,128)(2,1)S(1)} %fusion.18, s32[1024]{0:T(1024)S(1)} %fusion.68), kind=kCustom, calls=%fused_computation | custom fusion | bytes 8392704 | tf_op jit(solution)/shard_map/gather | solution.py:170
  98.9 2.5 broadcast_select_fusion.4
  101.4 98.7 %all_to_all.10 = bf16[16,64,2048]{2,1,0:T(8,128)(2,1)S(1)} all-to-all(bf16[16,64,2048]{2,1,0:T(8,128)(2,1)S(1)} %broadcast_select_fusion.4), channel_id=1, replica_groups=mesh['grp'=2,'sp'=4,'tp'=4] {'sp','tp'}, dimensions={0} | all-to-all | bytes 8388608 | tf_op jit(solution)/shard_map/all_to_all | solution.py:173
  200.1 2.0 copy-done.3
  202.1 3.7 %fusion.6 = f32[1024,512]{1,0:T(8,128)} fusion(bf16[1024,2048]{1,0:T(8,128)(2,1)S(1)} %bitcast.155, bf16[1,2048,512]{2,1,0:T(8,128)(2,1)S(1)} %copy-done.13), kind=kOutput, calls=%fused_computation.21 | convolution fusion | flops 2147483648 | bytes 8388608 | tf_op jit(solution)/shard_map/dot_general | solution.py:49
  205.8 10.1 %convolution_convert_fusion = bf16[1024,2048]{1,0:T(8,128)(2,1)} fusion(bf16[1,512,2048]{2,1,0:T(8,128)(2,1)S(1)} %copy-done, f32[1024,512]{1,0:T(8,128)} %fusion.6, bf16[1024,2048]{1,0:T(8,128)(2,1)} %bitcast.156, bf16[1,2048,512]{2,1,0:T(8,128)(2,1)} %param.27), kind=kOutput, calls=%fused_computation.18 | convolution fusion | flops 4300210176 | bytes 14680064 | tf_op jit(solution)/shard_map/dot_general | solution.py:51
  215.8 5.4 %all-to-all-start.1 = ((bf16[16,64,2048]{2,1,0:T(8,128)(2,1)}), bf16[16,64,2048]{2,1,0:T(8,128)(2,1)}, u32[]{:S(2)}, u32[]{:S(2)}) async-start(bf16[16,64,2048]{2,1,0:T(8,128)(2,1)} %bitcast.154), calls=%async_computation.2 | async-start | bytes 8388608 | tf_op jit(solution)/shard_map/all_to_all | solution.py:178
  221.4 92.3 %all-to-all-done.1 = bf16[16,64,2048]{2,1,0:T(8,128)(2,1)} async-done(((bf16[16,64,2048]{2,1,0:T(8,128)(2,1)}), bf16[16,64,2048]{2,1,0:T(8,128)(2,1)}, u32[]{:S(2)}, u32[]{:S(2)}) %all-to-all-start.1) | async-done | bytes 4194336 | tf_op jit(solution)/shard_map/all_to_all | solution.py:178
  313.7 6.1 %gather_fusion.1 = bf16[256,2048]{1,0:T(8,128)(2,1)} fusion(bf16[1024,2048]{1,0:T(8,128)(2,1)} %bitcast.32, s32[1024]{0:T(1024)S(1)} %pad_clamp_fusion), kind=kCustom, calls=%fused_computation.1 | custom fusion | bytes 2098176 | tf_op jit(solution)/shard_map/gather | solution.py:179
  319.7 3.4 %reshape.418 = f32[128,2,2048]{2,1,0:T(2,128)} reshape(bf16[256,2048]{1,0:T(8,128)(2,1)} %gather_fusion.1) | data formatting | bytes 3145728 | tf_op jit(solution)/shard_map/convert_element_type | solution.py:180
  323.1 4.9 %multiply_reduce_fusion = f32[128,2048]{1,0:T(8,128)S(1)} fusion(f32[128,2,2048]{2,1,0:T(2,128)} %reshape.418, f32[128,2]{1,0:T(8,128)S(1)} %copy.59), kind=kLoop, calls=%fused_computation.25 | loop fusion | flops 786432 | bytes 3146752 | tf_op jit(solution)/shard_map/reduce_sum | solution.py:182
  328.0 1.0 fusion.19
  (81 shorter events, 2.1 us)
Async XLA Ops:
  6.5 199.2 %copy-start = (bf16[1,512,2048]{2,1,0:T(8,128)(2,1)S(1)}, bf16[1,512,2048]{2,1,0:T(8,128)(2,1)}, u32[]{:S(2)}) copy-start(bf16[1,512,2048]{2,1,0:T(8,128)(2,1)} %param.29) | copy-start | bytes 6291460
  6.5 39.1 %all-gather.4.cloned.1.call-start = ((), (), s32[]{:S(2)}) async-start(), calls=%async_computation.3 | async-start | bytes 1310720 | tf_op jit(solution)/shard_map/all_gather | solution.py:19
  10.7 4.3 %copy-start.4 = (bf16[4,128,2,128]{1,3,0,2:T(8,128)(2,1)}, bf16[4,128,2,128]{1,3,0,2:T(8,128)(2,1)S(1)}, u32[]{:S(2)}) copy-start(bf16[4,128,2,128]{1,3,0,2:T(8,128)(2,1)S(1)} %copy.44) | copy-start | bytes 786436
  12.8 4.1 %copy-start.14 = (u32[32]{0:T(128)S(1)}, u32[32]{0:T(128)}, u32[]{:S(2)}) copy-start(u32[32]{0:T(128)} %constant.100) | copy-start | bytes 388
  12.8 15.0 %copy-start.11 = (f32[512]{0:T(512)S(1)}, f32[512]{0:T(512)}, u32[]{:S(2)}) copy-start(f32[512]{0:T(512)} %param.21) | copy-start | bytes 6148
  16.8 73.5 %reduce-scatter.2.cloned.1.call-start = ((), (), s32[]{:S(2)}) async-start(), calls=%async_computation.4 | async-start | bytes 2621440 | tf_op jit(solution)/shard_map/reduce_scatter | solution.py:142
  51.0 1.5 copy-start.7
  51.1 1.4 copy-start.5
  52.5 2.4 copy-start.6
  55.0 2.5 copy-start.12
  60.1 0.7 copy-start.9
  60.1 30.2 %copy-start.1 = (bf16[128,2048]{1,0:T(8,128)(2,1)S(1)}, bf16[128,2048]{1,0:T(8,128)(2,1)}, u32[]{:S(2)}) copy-start(bf16[128,2048]{1,0:T(8,128)(2,1)} %param.23) | copy-start | bytes 1572868
  60.1 31.5 %copy-start.8 = (f32[2048]{0:T(1024)S(1)}, f32[2048]{0:T(1024)}, u32[]{:S(2)}) copy-start(f32[2048]{0:T(1024)} %param.24) | copy-start | bytes 24580
  101.4 100.6 %copy-start.13 = (bf16[1,2048,512]{2,1,0:T(8,128)(2,1)S(1)}, bf16[1,2048,512]{2,1,0:T(8,128)(2,1)}, u32[]{:S(2)}) copy-start(bf16[1,2048,512]{2,1,0:T(8,128)(2,1)} %param.28) | copy-start | bytes 6291460
  200.1 2.0 copy-start.3
  215.8 5.4 %copy-start.10 = (f32[128,2]{0,1:T(2,128)S(1)}, f32[128,2]{0,1:T(2,128)}, u32[]{:S(2)}) copy-start(f32[128,2]{0,1:T(2,128)} %param.26) | copy-start | bytes 3076
  215.8 97.8 %all-to-all-start.1 = ((bf16[16,64,2048]{2,1,0:T(8,128)(2,1)}), bf16[16,64,2048]{2,1,0:T(8,128)(2,1)}, u32[]{:S(2)}, u32[]{:S(2)}) async-start(bf16[16,64,2048]{2,1,0:T(8,128)(2,1)} %bitcast.154), calls=%async_computation.2 | async-start | bytes 8388608 | tf_op jit(solution)/shard_map/all_to_all | solution.py:178
  323.1 4.9 %copy-start.2 = (bf16[128,2048]{1,0:T(8,128)(2,1)S(1)}, bf16[128,2048]{1,0:T(8,128)(2,1)}, u32[]{:S(2)}) copy-start(bf16[128,2048]{1,0:T(8,128)(2,1)} %reduce-scatter.2.cloned.1.call-done) | copy-start | bytes 1572868
Sparse Core Ops, SparseCore 0:
  16.9 28.6 all-gather.3
  60.3 29.9 reduce-scatter.1
where the time goes:
time: 337 us; the launch traced here: 336 us
  waiting for transfers between devices  134 us (40%)
  blocking collectives  106 us (31%)
  local copies, waits for them, and re-layouts  30.9 us (9%)
  matrix products  23 us (7%)
  other arithmetic  22.1 us (7%)
  between operations  14.4 us (4%)
  starting transfers between devices  5.41 us (2%)
    all_to_all x1, blocking collectives, per_device(): lax.all_to_all(outgoing, ('sp', 'tp'), split_axis=0, concat_axis=0, tiled...  98.7 us
    all_to_all x1, waiting for transfers between devices, per_device(): lax.all_to_all(served, ('sp', 'tp'), split_axis=0, concat_axis=0, tiled=T...  92.3 us
    reduce_scatter x1, waiting for transfers between devices, per_device(): lax.psum_scatter(jnp.dot(mixed, out_weight, preferred_element_type=jnp.fl...  27.1 us
    all_gather x1, waiting for transfers between devices, entering(): everything = jax.tree.map(lambda part: lax.all_gather(part, axis), x)  14.6 us
    dot_general x1, matrix products, expert_ffn(): jnp.dot(hidden, down_weight[0], preferred_element_type=jnp.float32)  10.1 us
    unnamed x1, blocking collectives  7.23 us
  transfers between devices with their start and end apart: 3, of which 3 were waited for; matrix products, arithmetic and copies ran while one was open for 3% of the time, Pallas kernels for 0%

commit v1 on v0

--- a/solution.py
+++ b/solution.py
@@ -1,6 +1,10 @@
+import functools
+
 import jax
 import jax.numpy as jnp
 from jax import lax
+from jax.experimental import pallas as pl
+from jax.experimental.pallas import tpu as pltpu
 from jax.sharding import PartitionSpec as P
 
 QK_HEAD = 128
@@ -52,6 +56,244 @@
         jnp.bfloat16
     )
     return output.reshape(arrived.shape)
+
+
+MESH = pl.DeviceIdType.MESH
+LANES = 128
+PAIR = 2
+VMEM_BUDGET = 40 * 2**20
+
+
+def flip(index, bits, count):
+    out, step = index, 1
+    while step < count:
+        if bits & step:
+            out = out + step * (1 - 2 * ((index // step) % 2))
+        step *= 2
+    return out
+
+
+def moe_kernel(
+    n_sp,
+    piece_ref,
+    mid_ref,
+    gate_ref,
+    up_ref,
+    down_ref,
+    out_ref,
+    buf,
+    hid,
+    mine,
+    sib_out,
+    sib_in,
+    x_out,
+    x_in,
+    z_out,
+    z_in,
+    keep,
+    ag_recv,
+    ag_z,
+    ag_x,
+    ag_s,
+    s_send,
+    s_recv,
+    x_send,
+    x_recv,
+    z_send,
+    z_recv,
+    own_sem,
+):
+    rows, width = mid_ref.shape
+    ff = gate_ref.shape[1]
+    z = lax.axis_index("sp")
+    t = lax.axis_index("tp")
+    x, c = t // PAIR, t % PAIR
+    ox, oc = 1 - x, 1 - c
+    expert = z * lax.axis_size("tp") + t
+    experts = n_sp * lax.axis_size("tp")
+    sib = {"tp": x * PAIR + oc}
+    part = {"tp": ox * PAIR + c}
+
+    def line(d):
+        return {"sp": flip(z, d, n_sp)}
+
+    barrier = pltpu.get_barrier_semaphore()
+    peers = [sib, part] + [line(d) for d in range(1, n_sp)]
+    for peer in peers:
+        pl.semaphore_signal(barrier, inc=1, device_id=peer, device_id_type=MESH)
+    pl.semaphore_wait(barrier, len(peers))
+
+    def remote(src, dst, send, recv, peer):
+        return pltpu.make_async_remote_copy(
+            src_ref=src, dst_ref=dst, send_sem=send, recv_sem=recv, device_id=peer, device_id_type=MESH
+        )
+
+    def slot(zz, xx, cc):
+        return buf.at[zz * PAIR + xx, cc]
+
+    def arrived(zz, xx, cc):
+        ref = slot(zz, xx, cc)
+        sem = ag_recv.at[zz * PAIR + xx, cc]
+        pltpu.make_async_copy(ref, ref, sem).wait()
+
+    def send_ag(src, zz, xx, sem, peer):
+        copy = remote(src, slot(zz, xx, c), sem, ag_recv.at[zz * PAIR + xx, c], peer)
+        copy.start()
+        return copy
+
+    pending = []
+    own = pltpu.make_async_copy(piece_ref, slot(z, x, c), own_sem)
+    own.start()
+    pending.append(send_ag(piece_ref, z, x, ag_x.at[0], part))
+    for d in range(1, n_sp):
+        pending.append(send_ag(piece_ref, z, x, ag_z.at[d], line(d)))
+    pending.append(send_ag(piece_ref, z, x, ag_s.at[0, 0], sib))
+    own.wait()
+
+    def forward(d):
+        zz = flip(z, d, n_sp)
+        arrived(zz, x, c)
+        pending.append(send_ag(slot(zz, x, c), zz, x, ag_x.at[d], part))
+        pending.append(send_ag(slot(zz, x, c), zz, x, ag_s.at[d, 0], sib))
+
+    lane = lax.broadcasted_iota(jnp.int32, (rows, LANES), 1)
+
+    def compute(pair):
+        for i in range(0, ff, 256):
+            a = buf[pair, :, :, :width].reshape(PAIR * rows, width)
+            g = jnp.dot(a, gate_ref[:, i : i + 256], preferred_element_type=jnp.float32)
+            u = jnp.dot(a, up_ref[:, i : i + 256], preferred_element_type=jnp.float32)
+            hid[:, i : i + 256] = (jax.nn.silu(g) * u).astype(jnp.bfloat16)
+
+    def weight(pair, cc):
+        w = buf[pair, cc, :, width:].astype(jnp.float32)
+        chosen = (lane == expert) | (lane == expert + experts)
+        return jnp.sum(jnp.where(chosen, w, 0.0), axis=1, keepdims=True)
+
+    def down(pair):
+        w_mine, w_sib = weight(pair, c), weight(pair, oc)
+        h_mine = hid[pl.ds(pl.multiple_of(c * rows, rows), rows), :]
+        h_sib = hid[pl.ds(pl.multiple_of(oc * rows, rows), rows), :]
+        both = jnp.concatenate([h_mine, h_sib], axis=0)
+        for j in range(0, width, 512):
+            o = jnp.dot(both, down_ref[:, j : j + 512], preferred_element_type=jnp.float32)
+            mine[:, j : j + 512] = o[:rows] * w_mine
+            sib_out[pair, :, j : j + 512] = (o[rows:] * w_sib).astype(jnp.bfloat16)
+
+    def exchange(pair):
+        copy = remote(sib_out.at[pair], sib_in.at[pair], s_send.at[pair], s_recv.at[pair], sib)
+        copy.start()
+        copy.wait()
+
+    def step_own(d):
+        zz = flip(z, d, n_sp)
+        arrived(zz, x, oc)
+        pair = zz * PAIR + x
+        compute(pair)
+        down(pair)
+        exchange(pair)
+        keep[d] = mine[...] + sib_in[pair].astype(jnp.float32)
+
+    def step_other(d):
+        zz = flip(z, d, n_sp)
+        arrived(zz, ox, c)
+        copy = send_ag(slot(zz, ox, c), zz, ox, ag_s.at[d, 1], sib)
+        pending.append(copy)
+        arrived(zz, ox, oc)
+        pair = zz * PAIR + ox
+        compute(pair)
+        down(pair)
+        exchange(pair)
+        x_out[d] = (mine[...] + sib_in[pair].astype(jnp.float32)).astype(jnp.bfloat16)
+        copy = remote(x_out.at[d], x_in.at[d], x_send.at[d], x_recv.at[d], part)
+        copy.start()
+        return copy
+
+    def finish(d, copy):
+        copy.wait()
+        total = keep[d] + x_in[d].astype(jnp.float32)
+        if d == 0:
+            keep[0] = total
+            return
+        z_out[d] = total.astype(jnp.bfloat16)
+        back = remote(z_out.at[d], z_in.at[d], z_send.at[d], z_recv.at[d], line(d))
+        back.start()
+        returns.append((d, back))
+
+    returns, crossed = [], []
+    for d in range(n_sp):
+        step_own(d)
+        if d + 1 < n_sp:
+            forward(d + 1)
+        crossed.append(step_other(d))
+        if d > 0:
+            finish(d - 1, crossed[d - 1])
+    finish(n_sp - 1, crossed[n_sp - 1])
+    total = keep[0]
+    for d, back in returns:
+        back.wait()
+        total = total + z_in[d].astype(jnp.float32)
+    out_ref[...] = (mid_ref[...].astype(jnp.float32) + total).astype(jnp.bfloat16)
+    for copy in pending:
+        copy.wait_send()
+
+
+def moe_bytes(rows, width, n_sp, n_tp):
+    return n_sp * n_tp * rows * width * 2 * 3
+
+
+def moe(piece, mid, gate_weight, up_weight, down_weight):
+    n_sp = lax.axis_size("sp")
+    rows, width = mid.shape
+    pairs = n_sp * PAIR
+    ff = gate_weight.shape[-1]
+    bf, f32 = jnp.bfloat16, jnp.float32
+    dma = pltpu.SemaphoreType.DMA
+    return pl.pallas_call(
+        functools.partial(moe_kernel, n_sp),
+        out_shape=jax.ShapeDtypeStruct((rows, width), bf),
+        in_specs=[pl.BlockSpec(memory_space=pltpu.VMEM)] * 5,
+        out_specs=pl.BlockSpec(memory_space=pltpu.VMEM),
+        scratch_shapes=[
+            pltpu.VMEM((pairs, PAIR, rows, piece.shape[1]), bf),
+            pltpu.VMEM((PAIR * rows, ff), bf),
+            pltpu.VMEM((rows, width), f32),
+            pltpu.VMEM((pairs, rows, width), bf),
+            pltpu.VMEM((pairs, rows, width), bf),
+            pltpu.VMEM((n_sp, rows, width), bf),
+            pltpu.VMEM((n_sp, rows, width), bf),
+            pltpu.VMEM((n_sp, rows, width), bf),
+            pltpu.VMEM((n_sp, rows, width), bf),
+            pltpu.VMEM((n_sp, rows, width), f32),
+            dma((pairs, PAIR)),
+            dma((n_sp,)),
+            dma((n_sp,)),
+            dma((n_sp, PAIR)),
+            dma((pairs,)),
+            dma((pairs,)),
+            dma((n_sp,)),
+            dma((n_sp,)),
+            dma((n_sp,)),
+            dma((n_sp,)),
+            dma,
+        ],
+        compiler_params=pltpu.CompilerParams(
+            collective_id=3, has_side_effects=True, vmem_limit_bytes=60 * 2**20
+        ),
+        name="moe",
+    )(piece, mid, gate_weight, up_weight, down_weight)
+
+
+def row_weights(expert_ids, expert_mix, experts):
+    share = expert_mix / jnp.sum(expert_mix, axis=1, keepdims=True)
+    names = jnp.arange(experts, dtype=jnp.int32)
+    dense = jnp.sum(
+        jnp.where(expert_ids[:, :, None] == names[None, None, :], share[:, :, None], 0.0), axis=1
+    )
+    high = lax.reduce_precision(dense, 8, 7)
+    low = dense - high
+    both = jnp.concatenate([high, low], axis=1).astype(jnp.bfloat16)
+    return jnp.pad(both, ((0, 0), (0, -both.shape[1] % LANES)))
 
 
 def per_device(
@@ -151,6 +393,12 @@
     ).astype(jnp.bfloat16)
     width = normed.shape[1]
     expert_group = lax.axis_size("sp") * lax.axis_size("tp")
+    n_sp, n_tp = lax.axis_size("sp"), lax.axis_size("tp")
+    if n_tp == PAIR * PAIR and moe_bytes(shard, width, n_sp, n_tp) <= VMEM_BUDGET:
+        piece = jnp.concatenate([normed, row_weights(expert_ids, expert_mix, expert_group)], axis=1)
+        return moe(
+            piece, mid_f.astype(jnp.bfloat16), gate_weight[0], up_weight[0], down_weight[0]
+        )
     assigns = expert_ids.reshape(-1)
     assign_count = assigns.shape[0]
     slots_each = CAP_FACTOR * assign_count // expert_group

time: 337 us -> 240 us (0.71)
  Pallas kernels: 0 us -> 137 us
  blocking collectives: 106 us -> 7.23 us
  waiting for transfers between devices: 134 us -> 43.9 us
  local copies, waits for them, and re-layouts: 30.9 us -> 13.3 us
  matrix products: 23 us -> 8.93 us
  other arithmetic: 22.1 us -> 13.6 us
  starting transfers between devices: 5.41 us -> 0.04 us
    pallas_call x0 -> x1, Pallas kernels: none -> 137 us  [moe(): pl.pallas_call(functools.partial(moe_kernel, n_sp), out_shape=jax.ShapeDt...]
    all_to_all x1 -> x0, blocking collectives: 98.7 us -> none  [per_device(): lax.all_to_all(outgoing, ('sp', 'tp'), split_axis=0, concat_axis=0, tiled...]
    all_to_all x1 -> x0, waiting for transfers between devices: 92.3 us -> none  [per_device(): lax.all_to_all(served, ('sp', 'tp'), split_axis=0, concat_axis=0, tiled=T...]
    dot_general x3 -> x0, matrix products: 14 us -> none  [the longest x1 10.1 us: expert_ffn(): jnp.dot(hidden, down_weight[0], preferred_element_type=jnp.float32)]
    gather x2 -> x0, local copies, waits for them, and re-layouts: 12.1 us -> none  [the longest x1 6.07 us: per_device(): picked = returned.reshape(expert_group * slots_each, width)[target]]
    all_to_all x1 -> x0, starting transfers between devices: 5.36 us -> none  [per_device(): lax.all_to_all(served, ('sp', 'tp'), split_axis=0, concat_axis=0, tiled=T...]
    reduce_sum x2, other arithmetic: 4.88 us -> 0.03 us  [the longest x1 0.02 us: row_weights(): share = expert_mix / jnp.sum(expert_mix, axis=1, keepdims=True)]
    convert_element_type x1 -> x0, local copies, waits for them, and re-layouts: 3.39 us -> none  [per_device(): picked = picked.reshape(shard, TOPK, width).astype(jnp.float32)]
  transfers between devices with their start and end apart: 3 -> 2, of which waited for: 3 -> 2; matrix products, arithmetic and copies ran while one was open for 3% -> 3% of each run, Pallas kernels for 0% -> 0%
where the time goes in v1:
time: 240 us; the launch traced here: 238 us
  Pallas kernels  137 us (57%)
  waiting for transfers between devices  43.9 us (18%)
  between operations  14.3 us (6%)
  other arithmetic  13.6 us (6%)
  local copies, waits for them, and re-layouts  13.3 us (6%)
  matrix products  8.93 us (4%)
  blocking collectives  7.23 us (3%)
    pallas_call x1, Pallas kernels, moe(): pl.pallas_call(functools.partial(moe_kernel, n_sp), out_shape=jax.ShapeDt...  137 us
    reduce_scatter x1, waiting for transfers between devices, per_device(): lax.psum_scatter(jnp.dot(mixed, out_weight, preferred_element_type=jnp.fl...  29.3 us
    all_gather x1, waiting for transfers between devices, entering(): everything = jax.tree.map(lambda part: lax.all_gather(part, axis), x)  14.6 us
    unnamed x1, blocking collectives  7.23 us
  transfers between devices with their start and end apart: 2, of which 2 were waited for; matrix products, arithmetic and copies ran while one was open for 3% of the time, Pallas kernels for 0%

profile of v1, /device:TPU:11, one launch (start us, length us, event | category | flops | bytes accessed | tf_op | source)
XLA Modules:
  0.0 238.4 jit_solution(17584522967002292421)
XLA Ops:
  6.5 0.9 fusion.53
  7.4 0.6 reduce_window_sum.13
  8.0 0.2 slice_reduce_fusion
  8.2 0.7 add.289
  8.9 0.2 fusion.54
  9.1 0.3 slice_reduce_fusion.6
  9.4 0.1 exponential_bitcast_fusion
  9.5 1.0 reshape.357
  10.5 0.2 copy.62
  10.7 2.1 reshape.358
  12.8 1.3 convolution_bitcast_fusion
  14.2 0.8 fusion.27
  15.0 1.8 copy.67
  16.9 0.7 dynamic-slice
  18.2 0.2 dynamic-update-slice
  18.5 0.2 dynamic-update-slice.1
  18.7 7.2 %all-reduce.3 = (f32[8]{0:T(128)S(1)}, f32[8]{0:T(128)S(1)}) all-reduce(f32[8]{0:T(128)S(1)} %dynamic-update-slice, f32[8]{0:T(128)S(1)} %dynamic-update-slice.1), channel_id=2, replica_groups=mesh['grp'=2,'sp'=4,'tp'=4] {'sp'}, use_global_device_ids=true, to_apply=%add.1 | all-reduce | flops 16 | bytes 128
  25.9 0.1 reshape.363
  26.0 0.1 reshape.364
  26.1 1.7 reshape.359
  27.9 0.4 fusion.23
  28.3 2.8 %fusion.7 = f32[2,4,128,256]{3,2,1,0:T(8,128)} fusion(bf16[4,128,2,128]{1,3,0,2:T(8,128)(2,1)} %copy-done.2, bf16[4,128,2,256]{3,2,1,0:T(2,128)(2,1)} %reshape.358, f32[2,4,128]{2,1,0:T(4,128)S(1)} %fusion.23, f32[2,4,128]{2,1,0:T(4,128)S(1)} %add.289, f32[2,4,128]{2,1,0:T(4,128)S(1)} %reduce_window_sum.13, pred[128,128]{1,0:T(8,128)(4,1)S(1)} %iota_compare_fusion.1, ...), kind=kOutput, calls=%fused_computation.21 | convolution fusion | flops 101580800 | bytes 2125824 | tf_op jit(solution)/shard_map/hcts,cshv->hctv/dot_general | solution.py:368
  31.0 14.6 %all-gather.4.cloned.1.call-done = f32[4,2,256,128]{3,2,1,0:T(8,128)} async-done(((f32[1,2,256,128]{3,2,1,0:T(8,128)}), f32[4,2,256,128]{3,2,1,0:T(8,128)}) %all-gather.4.cloned.1.call-update) | async-done | bytes 1048592 | tf_op jit(solution)/shard_map/all_gather | solution.py:23
  45.6 4.5 %while.18 = (s32[]{:T(128)}, f32[2]{0:T(128)S(1)}, f32[2,256,128]{2,1,0:T(8,128)S(1)}, f32[2]{0:T(128)S(1)}, s32[]{:T(128)}, /*index=5*/f32[4,2]{1,0:T(4,128)S(1...) while((s32[]{:T(128)}, f32[2]{0:T(128)S(1)}, ...), condition=%wide.region_4.5_spmd.clone, body=%wide.region_3.4_spmd.clone.sunk | while | flops 327704 | bytes 786671 | solution.py:33
  45.7 1.1 fusion.68
  46.8 1.1 fusion.68
  47.9 1.1 fusion.68
  49.1 1.1 fusion.68
  50.2 0.8 copy.73
  51.1 0.1 copy.75
  51.1 0.1 fusion.51
  51.2 1.2 fusion.61
  52.4 0.1 fusion.29
  52.5 2.2 multiply_reduce_fusion
  54.8 0.1 copy.68
  54.9 0.1 fusion.49
  55.0 2.0 fusion.15
  57.0 0.5 copy.76
  57.5 0.1 copy.83
  57.6 2.6 %convolution_convert_fusion = bf16[512,2048]{1,0:T(8,128)(2,1)} fusion(bf16[512,512]{1,0:T(8,128)(2,1)S(1)} %bitcast.140, bf16[512,2048]{1,0:T(8,128)(2,1)S(1)} %copy-done), kind=kOutput, calls=%fused_computation.14 | convolution fusion | flops 1074790400 | bytes 4718592 | tf_op jit(solution)/shard_map/dot_general | solution.py:385
  60.3 0.6 copy-done.7
  61.0 0.1 copy.77
  61.1 29.3 %reduce-scatter.2.cloned.1.call-done = bf16[128,2048]{1,0:T(8,128)(2,1)} async-done(((bf16[512,2048]{1,0:T(8,128)(2,1)}), bf16[128,2048]{1,0:T(8,128)(2,1)}) %reduce-scatter.2.cloned.1.call-update) | async-done | bytes 524304 | tf_op jit(solution)/shard_map/reduce_scatter | solution.py:384
  90.4 1.3 fusion.9
  91.8 0.2 fusion.11
  92.0 0.8 fusion.18.piece_ref
  92.8 136.9 %moe.1 = bf16[128,2048]{1,0:T(8,128)(2,1)} custom-call(bf16[128,2176]{1,0:T(8,128)(2,1)} %fusion.18.piece_ref, bf16[128,2048]{1,0:T(8,128)(2,1)} %copy-done.1, bf16[2048,512]{1,0:T(8,128)(2,1)} %bitcast.136, bf16[2048,512]{1,0:T(8,128)(2,1)} %bitcast.137, bf16[512,2048]{1,0:T(8,128)(2,1)} %bitcast.138), custom_call_target="tpu_custom_call" | custom-call | tf_op jit(solution)/shard_map/moe/pallas_call | solution.py:252
  229.7 1.9 copy.118
  (53 shorter events, 0.4 us)
Async XLA Ops:
  6.5 51.1 %copy-start = (bf16[512,2048]{1,0:T(8,128)(2,1)S(1)}, bf16[512,2048]{1,0:T(8,128)(2,1)}, u32[]{:S(2)}) copy-start(bf16[512,2048]{1,0:T(8,128)(2,1)} %param.22) | copy-start | bytes 6291460
  6.5 39.1 %all-gather.4.cloned.1.call-start = ((), (), s32[]{:S(2)}) async-start(), calls=%async_computation.1 | async-start | bytes 1310720 | tf_op jit(solution)/shard_map/all_gather | solution.py:23
  10.7 4.3 %copy-start.2 = (bf16[4,128,2,128]{1,3,0,2:T(8,128)(2,1)}, bf16[4,128,2,128]{1,3,0,2:T(8,128)(2,1)S(1)}, u32[]{:S(2)}) copy-start(bf16[4,128,2,128]{1,3,0,2:T(8,128)(2,1)S(1)} %copy.62) | copy-start | bytes 786436
  12.8 4.1 %copy-start.10 = (u32[32]{0:T(128)S(1)}, u32[32]{0:T(128)}, u32[]{:S(2)}) copy-start(u32[32]{0:T(128)} %constant.69) | copy-start | bytes 388
  12.8 15.0 %copy-start.8 = (f32[512]{0:T(512)S(1)}, f32[512]{0:T(512)}, u32[]{:S(2)}) copy-start(f32[512]{0:T(512)} %param.21) | copy-start | bytes 6148
  16.8 73.6 %reduce-scatter.2.cloned.1.call-start = ((), (), s32[]{:S(2)}) async-start(), calls=%async_computation.2 | async-start | bytes 2621440 | tf_op jit(solution)/shard_map/reduce_scatter | solution.py:384
  51.0 1.5 copy-start.5
  51.1 1.4 copy-start.3
  60.3 0.7 copy-start.7
  60.3 0.7 copy-start.9
  60.3 30.2 %copy-start.4 = (bf16[128,2048]{1,0:T(8,128)(2,1)S(1)}, bf16[128,2048]{1,0:T(8,128)(2,1)}, u32[]{:S(2)}) copy-start(bf16[128,2048]{1,0:T(8,128)(2,1)} %param.23) | copy-start | bytes 1572868
  60.3 31.5 %copy-start.6 = (f32[2048]{0:T(1024)S(1)}, f32[2048]{0:T(1024)}, u32[]{:S(2)}) copy-start(f32[2048]{0:T(1024)} %param.24) | copy-start | bytes 24580
  91.7 1.1 copy-start.1
Sparse Core Ops, SparseCore 0:
  16.9 28.6 all-gather.3
  60.4 29.9 reduce-scatter.1
